TPU v7x, 32 devices: a whole 2x2x4 slice. The times are simulated.
32 devices in a mesh: sp: 8 (over z, x), tp: 4 (over y, core).
Axes of the slice: x: 2, y: 2, z: 4, core: 2. Of those that a mesh axis runs over, the one named last changes fastest.
Arguments:
- moe_in: bfloat16 [1536, 2048], P('sp', 'tp'), may hold values from -6 to 6
- cotangent: bfloat16 [1536, 2048], P('sp', 'tp'), may hold values from -6 to 6
- routes: int32 [1536, 2], P('sp'), may hold values from 0 to 7, all different within a row; in each aligned block of 192 rows (0 to 191, 192 to 383, ...) at most 60 rows name the same one
- route_weight: float32 [1536, 2], P('sp'), may hold values from 0.2 to 1
- w_gate: bfloat16 [8, 3584, 2048], P('sp', 'tp'), may hold values from -0.125 to 0.125
- w_up: bfloat16 [8, 3584, 2048], P('sp', 'tp'), may hold values from -0.125 to 0.125
- w_down: bfloat16 [8, 3584, 2048], P('sp', 'tp'), may hold values from -0.09375 to 0.09375
- conv_pre: bfloat16 [1536, 2048], P('sp', 'tp'), may hold values from -6 to 6
- norm_mean: float32 [1536], P('sp'), may hold values from -3 to 3
- norm_rstd: float32 [1536], P('sp'), may hold values from 0.5 to 2
- ln_gain: float32 [2048], P('tp'), may hold values from 0.1 to 1.9
- ln_shift: float32 [2048], P('tp'), may hold values from -3 to 3
- taps: float32 [31, 2048], P(None, 'tp'), may hold values from -1 to 1
- w_proj: bfloat16 [2048, 2048], P('sp', 'tp'), may hold values from -0.125 to 0.125
Outputs:
- grad_up: bfloat16 [8, 3584, 2048], P('sp', 'tp')
- grad_down: bfloat16 [8, 3584, 2048], P('sp', 'tp')
- grad_stream: bfloat16 [1536, 2048], P('sp', 'tp')
- grad_proj: float32 [2048, 2048], P('sp', 'tp')
- grad_conv: bfloat16 [1536, 2048], P('sp', 'tp')
Inputs may be any that keep to these rules, and one draw needn't show every extreme that they name: `routes`: each token names 2 different experts. Among the tokens of one index of sp no expert is named more than 60 times, a bound that some block reaches.
All inputs are finite; a program needn't handle non-finite values.
Results may differ from a plain program's by a relative error of at most 0.02.
Values may be sent and summed in bfloat16 or wider, within the bound.
A program may use at most 64 MiB of HBM per device.

v0:
```python
import jax
import jax.numpy as jnp
from jax import lax
from jax.sharding import PartitionSpec as P


def passed_along(value, axis, steps):
    count = lax.axis_size(axis)
    first, last = (max(0, -steps), min(count, count - steps))
    return lax.ppermute(value, axis, [(source, source + steps) for source in range(first, last)])


def silu_slope(pre_value, sigmoid_value):
    return sigmoid_value * (1.0 + pre_value * (1.0 - sigmoid_value))


def expert_backward(expert_rows, routed_rows, gate_weight, up_weight, down_weight):
    gate_pre = lax.dot_general(
        expert_rows, gate_weight, (((1,), (1,)), ((), ())), preferred_element_type=jnp.float32
    )
    up_pre = lax.dot_general(
        expert_rows, up_weight, (((1,), (1,)), ((), ())), preferred_element_type=jnp.float32
    )
    gate_sigmoid = jax.nn.sigmoid(gate_pre)
    gate_active = gate_pre * gate_sigmoid
    hidden = (gate_active * up_pre).astype(jnp.bfloat16)
    hidden_grad = lax.dot_general(
        routed_rows, down_weight, (((1,), (1,)), ((), ())), preferred_element_type=jnp.float32
    )
    grad_down = lax.dot_general(
        hidden, routed_rows, (((0,), (0,)), ((), ())), preferred_element_type=jnp.float32
    ).astype(jnp.bfloat16)
    gate_grad = (hidden_grad * up_pre * silu_slope(gate_pre, gate_sigmoid)).astype(jnp.bfloat16)
    up_grad = (hidden_grad * gate_active).astype(jnp.bfloat16)
    grad_up = lax.dot_general(
        up_grad, expert_rows, (((0,), (0,)), ((), ())), preferred_element_type=jnp.float32
    ).astype(jnp.bfloat16)
    partial_rows = jnp.dot(gate_grad, gate_weight, preferred_element_type=jnp.float32)
    partial_rows = partial_rows + jnp.dot(up_grad, up_weight, preferred_element_type=jnp.float32)
    return (grad_up[None], grad_down[None], partial_rows)


def on_device(
    moe_in,
    cotangent,
    routes,
    route_weight,
    w_gate,
    w_up,
    w_down,
    conv_pre,
    norm_mean,
    norm_rstd,
    ln_gain,
    ln_shift,
    taps,
    w_proj,
):
    devices = lax.axis_size("sp")
    local_tokens = routes.shape[0]
    top_count = routes.shape[1]
    channels = moe_in.shape[1]
    capacity = 5 * local_tokens // (2 * devices)
    route_ids = routes.reshape(-1)
    onehot = (route_ids[:, None] == jnp.arange(devices, dtype=jnp.int32)[None, :]).astype(jnp.int32)
    earlier = jnp.cumsum(onehot, axis=0) - onehot
    targets = route_ids * capacity + jnp.sum(earlier * onehot, axis=1)
    positions = jnp.arange(devices * capacity, dtype=jnp.int32)
    matches = targets[None, :] == positions[:, None]
    filled = jnp.any(matches, axis=1)[:, None]
    pair_index = jnp.arange(targets.shape[0], dtype=jnp.int32)
    route_of_slot = jnp.sum(jnp.where(matches, pair_index[None, :], 0), axis=1)
    zero_value = jnp.zeros((), jnp.bfloat16)
    routed = (route_weight[:, :, None] * cotangent.astype(jnp.float32)[:, None, :]).astype(
        jnp.bfloat16
    )
    routed = routed.reshape(local_tokens * top_count, cotangent.shape[1])
    send_rows = jnp.where(filled, jnp.take(moe_in, route_of_slot // top_count, axis=0), zero_value)
    send_routed = jnp.where(filled, jnp.take(routed, route_of_slot, axis=0), zero_value)
    send_rows, send_routed = (send_rows, send_routed)
    part_rows, part_routed = (
        lax.all_to_all(send_rows, "sp", split_axis=0, concat_axis=0, tiled=True),
        lax.all_to_all(send_routed, "sp", split_axis=0, concat_axis=0, tiled=True),
    )
    expert_rows, routed_rows = (
        lax.all_gather(part_rows, "tp", axis=1, tiled=True),
        lax.all_gather(part_routed, "tp", axis=1, tiled=True),
    )
    grad_up, grad_down, partial_rows = expert_backward(
        expert_rows, routed_rows, w_gate[0], w_up[0], w_down[0]
    )
    shared = lax.psum_scatter(
        partial_rows.astype(jnp.bfloat16).astype(jnp.float32).astype(jnp.bfloat16),
        "tp",
        scatter_dimension=1,
        tiled=True,
    )
    returned = lax.all_to_all(shared, "sp", split_axis=0, concat_axis=0, tiled=True)
    picked = jnp.take(returned, targets, axis=0).astype(jnp.float32)
    grad_stream = (
        cotangent.astype(jnp.float32)
        + jnp.sum(picked.reshape(local_tokens, top_count, returned.shape[1]), axis=1)
    ).astype(jnp.bfloat16)
    mix_grad = lax.all_gather(grad_stream, "tp", axis=1, tiled=True)
    normed = (conv_pre.astype(jnp.float32) - norm_mean[:, None]) * norm_rstd[:, None]
    pre_act = normed * ln_gain[None, :] + ln_shift[None, :]
    act_sigmoid = jax.nn.sigmoid(pre_act)
    activated = (pre_act * act_sigmoid).astype(jnp.bfloat16)
    columns = mix_grad
    act_grad = jnp.dot(
        columns,
        lax.all_gather(w_proj, "sp", axis=0, tiled=True),
        preferred_element_type=jnp.float32,
    )
    columns = mix_grad
    grad_proj = lax.psum_scatter(
        lax.dot_general(
            columns, activated, (((0,), (0,)), ((), ())), preferred_element_type=jnp.float32
        ).astype(jnp.bfloat16),
        "sp",
        scatter_dimension=0,
        tiled=True,
    ).astype(jnp.float32)
    normed_grad = act_grad * silu_slope(pre_act, act_sigmoid) * ln_gain[None, :]
    first_sum, second_sum = lax.psum(
        (jnp.sum(normed_grad, axis=1), jnp.sum(normed_grad * normed, axis=1)), "tp"
    )
    width = channels * lax.axis_size("tp")
    conv_grad = norm_rstd[:, None] * (
        normed_grad - first_sum[:, None] / width - normed * (second_sum[:, None] / width)
    )
    lag_count = taps.shape[0]
    rim_rows = passed_along(conv_grad[: lag_count - 1], "sp", -1)
    extended = jnp.concatenate([conv_grad, rim_rows], axis=0)
    grad_conv = jnp.zeros((local_tokens, channels), jnp.float32)
    for lag in range(lag_count):
        grad_conv = grad_conv + taps[lag][None, :] * extended[lag : lag + local_tokens]
    return (grad_up, grad_down, grad_stream, grad_proj, grad_conv.astype(jnp.bfloat16))


def solution(mesh):
    placed = (
        P("sp", "tp"),
        P("sp", "tp"),
        P("sp", None),
        P("sp", None),
        P("sp", "tp", None),
        P("sp", "tp", None),
        P("sp", "tp", None),
        P("sp", "tp"),
        P("sp"),
        P("sp"),
        P("tp"),
        P("tp"),
        P(None, "tp"),
        P("sp", "tp"),
    )
    return jax.shard_map(
        on_device,
        mesh=mesh,
        in_specs=placed,
        out_specs=(
            P("sp", "tp", None),
            P("sp", "tp", None),
            P("sp", "tp"),
            P("sp", "tp"),
            P("sp", "tp"),
        ),
        check_vma=False,
    )
```

profile of v0, /device:TPU:0, one launch (start us, length us, event | category | flops | bytes accessed | tf_op | source)
XLA Modules:
  0.0 252.3 jit_solution(15839050493758933226)
XLA Ops:
  8.1 0.8 copy.28
  9.2 0.9 reduce-window.6
  10.0 0.2 slice_reduce_fusion
  10.4 0.2 select_reduce_fusion
  10.6 0.2 fusion.15
  10.8 1.1 mul.435
  12.0 0.5 mul.436
  12.7 0.1 mul.433
  12.9 2.1 gather_fusion
  15.2 2.1 gather_fusion.1
  17.5 0.3 select_select_fusion
  17.8 21.6 %all_to_all.30 = bf16[8,60,512]{2,1,0:T(8,128)(2,1)S(1)} all-to-all(bf16[8,60,512]{2,1,0:T(8,128)(2,1)S(1)} %get-tuple-element.44), channel_id=1, replica_groups=mesh['sp'=8,'tp'=4] {'sp'}, dimensions={0} | all-to-all | bytes 983040 | tf_op jit(solution)/shard_map/all_to_all | solution.py:82
  39.4 0.9 all_to_all.23
  40.4 17.5 %all_to_all.31 = bf16[8,60,512]{2,1,0:T(8,128)(2,1)S(1)} all-to-all(bf16[8,60,512]{2,1,0:T(8,128)(2,1)S(1)} %get-tuple-element.45), channel_id=1, replica_groups=mesh['sp'=8,'tp'=4] {'sp'}, dimensions={0} | all-to-all | bytes 983040 | tf_op jit(solution)/shard_map/all_to_all | solution.py:83
  57.9 0.9 all_to_all.21
  58.8 0.2 reduce-scatter.3.cloned.1.call-start
  59.0 2.3 all-gather.6.cloned.1.call-done
  61.4 4.9 %fusion.6 = f32[480,896]{1,0:T(8,128)S(1)} fusion(bf16[480,2048]{1,0:T(8,128)(2,1)} %all-gather.6.cloned.1.call-done, bf16[1,896,2048]{2,1,0:T(8,128)(2,1)} %param.18), kind=kOutput, calls=%fused_computation.39 | convolution fusion | flops 1761607680 | bytes 7356416 | tf_op jit(solution)/shard_map/dot_general | solution.py:18
  66.2 19.1 %all-gather.4.cloned.1.call-done = bf16[480,2048]{1,0:T(8,128)(2,1)} async-done(((bf16[480,512]{1,0:T(8,128)(2,1)}), bf16[480,2048]{1,0:T(8,128)(2,1)}) %all-gather.4.cloned.1.call-update) | async-done | bytes 1966096 | tf_op jit(solution)/shard_map/all_gather | solution.py:87
  85.4 5.1 %multiply_convert_fusion.2 = (bf16[480,896]{1,0:T(8,128)(2,1)S(1)}, f32[480,896]{1,0:T(8,128)S(1)}) fusion(f32[480,896]{1,0:T(8,128)S(1)} %fusion.6, bf16[480,2048]{1,0:T(8,128)(2,1)} %all-gather.4.cloned.1.call-done, bf16[1,896,2048]{2,1,0:T(8,128)(2,1)} %param.20), kind=kOutput, calls=%fused_computation.48 | convolution fusion | flops 1764188160 | bytes 9936896 | tf_op jit(solution)/shard_map/dot_general | solution.py:27
  90.5 0.9 copy-done.17
  91.4 2.2 fusion
  93.6 2.3 fusion.2
  95.9 1.2 copy-done.16
  97.1 3.7 %add_convert_fusion = bf16[480,2048]{1,0:T(8,128)(2,1)} fusion(f32[480,2048]{1,0:T(8,128)S(1)} %fusion, bf16[1,896,2048]{2,1,0:T(8,128)(2,1)S(1)} %copy-done.10, f32[480,896]{1,0:T(8,128)S(1)} %fusion.6, f32[480,896]{1,0:T(8,128)S(1)} %get-tuple-element.47, f32[480,896]{1,0:T(8,128)S(1)} %fusion.2), kind=kOutput, calls=%fused_computation.32 | convolution fusion | flops 1767874560 | bytes 14729216 | tf_op jit(solution)/shard_map/dot_general | solution.py:38
  100.9 0.5 all-gather.8.cloned.1.call-update
  101.4 30.0 %reduce-scatter.3.cloned.1.call-done = bf16[480,512]{1,0:T(8,128)(2,1)} async-done(((bf16[480,2048]{1,0:T(8,128)(2,1)}), bf16[480,512]{1,0:T(8,128)(2,1)}) %reduce-scatter.3.cloned.1.call-update) | async-done | bytes 491536 | tf_op jit(solution)/shard_map/reduce_scatter | solution.py:92
  131.4 1.9 all_to_all.24
  133.3 5.5 %all-to-all-start.2 = ((bf16[8,60,512]{2,1,0:T(8,128)(2,1)}), bf16[8,60,512]{2,1,0:T(8,128)(2,1)S(1)}, u32[]{:S(2)}, u32[]{:S(2)}) async-start(bf16[8,60,512]{2,1,0:T(8,128)(2,1)} %all_to_all.24), calls=%async_computation.3 | async-start | bytes 1048576 | tf_op jit(solution)/shard_map/all_to_all | solution.py:98
  139.2 0.1 mul.447
  139.4 0.2 copy.32
  139.6 21.8 %all-to-all-done.2 = bf16[8,60,512]{2,1,0:T(8,128)(2,1)S(1)} async-done(((bf16[8,60,512]{2,1,0:T(8,128)(2,1)}), bf16[8,60,512]{2,1,0:T(8,128)(2,1)S(1)}, u32[]{:S(2)}, u32[]{:S(2)}) %all-to-all-start.2) | async-done | bytes 491552 | tf_op jit(solution)/shard_map/all_to_all | solution.py:98
  161.5 2.1 gather_fusion.2
  163.6 0.2 gather.23
  163.8 1.1 convert_reduce_fusion
  165.0 8.4 %all_gather.14 = bf16[192,2048]{1,0:T(8,128)(2,1)S(1)} all-gather(bf16[192,512]{1,0:T(8,128)(2,1)S(1)} %add_convert_fusion.1), channel_id=1, replica_groups=mesh['sp'=8,'tp'=4] {'tp'}, dimensions={1}, use_global_device_ids=true | all-gather | bytes 983040 | tf_op jit(solution)/shard_map/all_gather | solution.py:104
  173.4 2.3 convolution_convert_fusion
  175.7 0.8 copy-done.4
  176.6 0.7 copy-done.12
  177.3 6.0 %convert_bitcast_fusion = bf16[1,896,2048]{2,1,0:T(8,128)(2,1)} fusion(bf16[480,2048]{1,0:T(8,128)(2,1)S(1)} %copy-done.12, f32[480,896]{1,0:T(8,128)} %copy-done.16, f32[480,896]{1,0:T(8,128)} %copy-done.15), kind=kOutput, calls=%fused_computation.43 | convolution fusion | flops 1766023168 | bytes 9076736 | tf_op jit(solution)/shard_map/dot_general | solution.py:30
  183.3 2.5 fusion.121
  185.8 7.0 %all-reduce = (f32[192]{0:T(256)S(1)}, f32[192]{0:T(256)S(1)}) all-reduce(f32[192]{0:T(256)S(1)} %get-tuple-element.6, f32[192]{0:T(256)S(1)} %get-tuple-element.5), channel_id=1, replica_groups=mesh['sp'=8,'tp'=4] {'tp'}, use_global_device_ids=true, to_apply=%region_11.12 | all-reduce | flops 384 | bytes 3072 | tf_op jit(solution)/shard_map/psum | solution.py:125
  192.7 0.2 subtract_multiply_fusion
  192.9 1.3 collective-permute-start
  194.2 5.5 %convert_bitcast_fusion.1 = bf16[1,896,2048]{2,1,0:T(8,128)(2,1)} fusion(bf16[480,896]{1,0:T(8,128)(2,1)S(1)} %copy-done.18, bf16[480,2048]{1,0:T(8,128)(2,1)} %all-gather.6.cloned.1.call-done), kind=kOutput, calls=%fused_computation.44 | convolution fusion | flops 1763442688 | bytes 6496256 | tf_op jit(solution)/shard_map/dot_general | solution.py:35
  199.8 2.5 fusion.20
  202.3 41.1 %reduce-scatter.5.cloned.1.call-done = bf16[256,512]{1,0:T(8,128)(2,1)} async-done(((bf16[2048,512]{1,0:T(8,128)(2,1)}), bf16[256,512]{1,0:T(8,128)(2,1)}) %reduce-scatter.5.cloned.1.call-update) | async-done | bytes 262160 | tf_op jit(solution)/shard_map/reduce_scatter | solution.py:116
  243.4 1.8 convert_element_type.72
  (73 shorter events, 2.0 us)
Async XLA Ops:
  8.0 7.2 %copy-start = (bf16[192,512]{1,0:T(8,128)(2,1)S(1)}, bf16[192,512]{1,0:T(8,128)(2,1)}, u32[]{:S(2)}) copy-start(bf16[192,512]{1,0:T(8,128)(2,1)} %param.14) | copy-start | bytes 589828
  8.0 4.5 %copy-start.6 = (f32[192,2]{0,1:T(2,128)S(1)}, f32[192,2]{0,1:T(2,128)}, u32[]{:S(2)}) copy-start(f32[192,2]{0,1:T(2,128)} %param.17) | copy-start | bytes 4612
  8.0 53.3 %all-gather.6.cloned.1.call-start = ((), (), s32[]{:S(2)}) async-start(), calls=%async_computation.6 | async-start | bytes 2457600 | tf_op jit(solution)/shard_map/all_gather | solution.py:86
  40.3 45.0 %all-gather.4.cloned.1.call-start = ((), (), s32[]{:S(2)}) async-start(), calls=%async_computation.5 | async-start | bytes 2457600 | tf_op jit(solution)/shard_map/all_gather | solution.py:87
  58.8 72.6 %reduce-scatter.3.cloned.1.call-start = ((), (), s32[]{:S(2)}) async-start(), calls=%async_computation.7 | async-start | bytes 2457600 | tf_op jit(solution)/shard_map/reduce_scatter | solution.py:92
  66.2 29.7 %copy-start.15 = (f32[480,896]{1,0:T(8,128)}, f32[480,896]{1,0:T(8,128)S(1)}, u32[]{:S(2)}) copy-start(f32[480,896]{1,0:T(8,128)S(1)} %fusion.6) | copy-start | bytes 5160964
  85.3 6.0 %copy-start.9 = (bf16[1,896,2048]{2,1,0:T(8,128)(2,1)S(1)}, bf16[1,896,2048]{2,1,0:T(8,128)(2,1)}, u32[]{:S(2)}) copy-start(bf16[1,896,2048]{2,1,0:T(8,128)(2,1)} %param.19) | copy-start | bytes 11010052
  90.5 0.9 copy-start.17
  91.4 2.2 copy-start.11
  93.6 3.5 %copy-start.10 = (bf16[1,896,2048]{2,1,0:T(8,128)(2,1)S(1)}, bf16[1,896,2048]{2,1,0:T(8,128)(2,1)}, u32[]{:S(2)}) copy-start(bf16[1,896,2048]{2,1,0:T(8,128)(2,1)} %param.18) | copy-start | bytes 11010052
  95.9 1.2 copy-start.16
  100.8 38.2 %copy-start.5 = (s32[192,2]{0,1:T(2,128)S(1)}, s32[192,2]{0,1:T(2,128)}, u32[]{:S(2)}) copy-start(s32[192,2]{0,1:T(2,128)} %param.16) | copy-start | bytes 4612
  100.9 82.4 %all-gather.8.cloned.1.call-start = ((), (), s32[]{:S(2)}) async-start(), calls=%async_computation.9 | async-start | bytes 2359296 | tf_op jit(solution)/shard_map/all_gather | solution.py:112
  133.3 28.1 %all-to-all-start.2 = ((bf16[8,60,512]{2,1,0:T(8,128)(2,1)}), bf16[8,60,512]{2,1,0:T(8,128)(2,1)S(1)}, u32[]{:S(2)}, u32[]{:S(2)}) async-start(bf16[8,60,512]{2,1,0:T(8,128)(2,1)} %all_to_all.24), calls=%async_computation.3 | async-start | bytes 1048576 | tf_op jit(solution)/shard_map/all_to_all | solution.py:98
  138.8 104.6 %reduce-scatter.5.cloned.1.call-start = ((), (), s32[]{:S(2)}) async-start(), calls=%async_computation.8 | async-start | bytes 2359296 | tf_op jit(solution)/shard_map/reduce_scatter | solution.py:116
  161.5 3.4 %copy-start.1 = (bf16[192,512]{1,0:T(8,128)(2,1)S(1)}, bf16[192,512]{1,0:T(8,128)(2,1)}, u32[]{:S(2)}) copy-start(bf16[192,512]{1,0:T(8,128)(2,1)} %param.15) | copy-start | bytes 589828
  163.6 9.8 %copy-start.3 = (bf16[192,512]{1,0:T(8,128)(2,1)S(1)}, bf16[192,512]{1,0:T(8,128)(2,1)}, u32[]{:S(2)}) copy-start(bf16[192,512]{1,0:T(8,128)(2,1)} %param.21) | copy-start | bytes 589828
  163.6 9.8 %copy-start.7 = (f32[192]{0:T(256)S(1)}, f32[192]{0:T(256)}, u32[]{:S(2)}) copy-start(f32[192]{0:T(256)} %param.23) | copy-start | bytes 2308
  163.6 9.8 %copy-start.8 = (f32[192]{0:T(256)S(1)}, f32[192]{0:T(256)}, u32[]{:S(2)}) copy-start(f32[192]{0:T(256)} %param.22) | copy-start | bytes 2308
  163.6 9.8 %copy-start.13 = (f32[512]{0:T(512)S(1)}, f32[512]{0:T(512)}, u32[]{:S(2)}) copy-start(f32[512]{0:T(512)} %param.25) | copy-start | bytes 6148
  163.6 9.8 %copy-start.14 = (f32[512]{0:T(512)S(1)}, f32[512]{0:T(512)}, u32[]{:S(2)}) copy-start(f32[512]{0:T(512)} %param.24) | copy-start | bytes 6148
  165.0 10.7 %copy-start.2 = (bf16[192,512]{1,0:T(8,128)(2,1)}, bf16[192,512]{1,0:T(8,128)(2,1)S(1)}, u32[]{:S(2)}) copy-start(bf16[192,512]{1,0:T(8,128)(2,1)S(1)} %add_convert_fusion.1) | copy-start | bytes 589828
  175.7 0.8 copy-start.4
  175.7 1.6 copy-start.12
  183.3 10.9 %copy-start.18 = (bf16[480,896]{1,0:T(8,128)(2,1)S(1)}, bf16[480,896]{1,0:T(8,128)(2,1)}, u32[]{:S(2)}) copy-start(bf16[480,896]{1,0:T(8,128)(2,1)} %copy-done.17) | copy-start | bytes 2580484
  192.9 6.9 %collective-permute-start = (f32[30,512]{1,0:T(8,128)S(1)}, f32[30,512]{1,0:T(8,128)S(1)}, u32[]{:S(2)}, u32[]{:S(2)}) collective-permute-start(f32[30,512]{1,0:T(8,128)S(1)} %slice.263), channel_id=1, source_target_pairs={{4,0},{8,4},{12,8},{16,12},{20,16},{24,20},{28,24},{5,1},{9,5},{13... | collective-permute-start | bytes 184328 | tf_op jit(solution)/shard_map/ppermute | solution.py:10
Sparse Core Ops, SparseCore 0:
  40.4 20.8 all-gather.5
  63.5 21.8 all-gather.3
  101.0 30.3 reduce-scatter.2
Sparse Core Ops, SparseCore 1:
  103.5 58.3 all-gather.7
  175.8 67.5 reduce-scatter.4
where the time goes:
time: 253 us; the launch traced here: 252 us
  waiting for transfers between devices  115 us (45%)
  blocking collectives  54.5 us (22%)
  matrix products  34.5 us (14%)
  local copies, waits for them, and re-layouts  18.2 us (7%)
  between operations  15.6 us (6%)
  other arithmetic  7.48 us (3%)
  starting transfers between devices  7.19 us (3%)
    reduce_scatter x1, waiting for transfers between devices, on_device(): lax.psum_scatter(lax.dot_general(columns, activated, (((0,), (0,)), ((),...  41.1 us
    reduce_scatter x1, waiting for transfers between devices, on_device(): lax.psum_scatter(partial_rows.astype(jnp.bfloat16).astype(jnp.float32).as...  30 us
    all_to_all x1, waiting for transfers between devices, on_device(): lax.all_to_all(shared, 'sp', split_axis=0, concat_axis=0, tiled=True)  21.8 us
    all_to_all x1, blocking collectives, on_device(): lax.all_to_all(send_rows, 'sp', split_axis=0, concat_axis=0, tiled=True)  21.6 us
    all_gather x1, waiting for transfers between devices, on_device(): lax.all_gather(part_routed, 'tp', axis=1, tiled=True)  19.1 us
    all_to_all x1, blocking collectives, on_device(): lax.all_to_all(send_routed, 'sp', split_axis=0, concat_axis=0, tiled=True)  17.5 us
    all_gather x1, blocking collectives, on_device(): mix_grad = lax.all_gather(grad_stream, 'tp', axis=1, tiled=True)  8.42 us
    psum x1, blocking collectives, on_device(): lax.psum((jnp.sum(normed_grad, axis=1), jnp.sum(normed_grad * normed, axi...  6.95 us
  transfers between devices with their start and end apart: 7, of which 5 were waited for; matrix products, arithmetic and copies ran while one was open for 11% of the time, Pallas kernels for 0%

commit v1 on v0

--- a/solution.py
+++ b/solution.py
@@ -2,6 +2,18 @@
 import jax.numpy as jnp
 from jax import lax
 from jax.sharding import PartitionSpec as P
+
+
+def sent_to_each(shard, axis, split, join):
+    ways, here = (lax.axis_size(axis), lax.axis_index(axis))
+    width = shard.shape[split] // ways
+    turned = jnp.roll(shard, -here * width, axis=split)
+    got = [lax.slice_in_dim(turned, 0, width, axis=split)]
+    for far in range(1, ways):
+        sent = lax.slice_in_dim(turned, far * width, (far + 1) * width, axis=split)
+        got.append(lax.ppermute(sent, axis, [(d, (d + far) % ways) for d in range(ways)]))
+    line = jnp.concatenate(got[::-1], axis=join)
+    return jnp.roll(line, (here + 1) * got[0].shape[join], axis=join)
 
 
 def passed_along(value, axis, steps):
@@ -80,7 +92,7 @@
     send_rows, send_routed = (send_rows, send_routed)
     part_rows, part_routed = (
         lax.all_to_all(send_rows, "sp", split_axis=0, concat_axis=0, tiled=True),
-        lax.all_to_all(send_routed, "sp", split_axis=0, concat_axis=0, tiled=True),
+        sent_to_each(send_routed, "sp", 0, 0),
     )
     expert_rows, routed_rows = (
         lax.all_gather(part_rows, "tp", axis=1, tiled=True),

time: 253 us -> 248 us (0.980)
  blocking collectives: 54.5 us -> 37 us
  starting transfers between devices: 7.19 us -> 16.2 us
  other arithmetic: 7.48 us -> 10.1 us
    all_to_all x1 -> x0, blocking collectives: 17.5 us -> none  [on_device(): lax.all_to_all(send_routed, 'sp', split_axis=0, concat_axis=0, tiled=True)]
    ppermute x0 -> x7, starting transfers between devices: none -> 9 us  [sent_to_each(): lax.ppermute(sent, axis, [(d, (d + far) % ways) for d in range(ways)])]
    ppermute x0 -> x7, waiting for transfers between devices: none -> 7.14 us  [sent_to_each(): lax.ppermute(sent, axis, [(d, (d + far) % ways) for d in range(ways)])]
  transfers between devices with their start and end apart: 7 -> 14, of which waited for: 5 -> 6; matrix products, arithmetic and copies ran while one was open for 11% -> 14% of each run, Pallas kernels for 0% -> 0%
where the time goes in v1:
time: 248 us
  waiting for transfers between devices  117 us (47%)
  blocking collectives  37 us (15%)
  matrix products  34.5 us (14%)
  local copies, waits for them, and re-layouts  17.2 us (7%)
  starting transfers between devices  16.2 us (7%)
  between operations  15.7 us (6%)
  other arithmetic  10.1 us (4%)
    reduce_scatter x1, waiting for transfers between devices, on_device(): lax.psum_scatter(lax.dot_general(columns, activated, (((0,), (0,)), ((),...  41 us
    reduce_scatter x1, waiting for transfers between devices, on_device(): lax.psum_scatter(partial_rows.astype(jnp.bfloat16).astype(jnp.float32).as...  30 us
    all_to_all x1, waiting for transfers between devices, on_device(): lax.all_to_all(shared, 'sp', split_axis=0, concat_axis=0, tiled=True)  21.8 us
    all_to_all x1, blocking collectives, on_device(): lax.all_to_all(send_rows, 'sp', split_axis=0, concat_axis=0, tiled=True)  21.6 us
    all_gather x1, waiting for transfers between devices, on_device(): lax.all_gather(part_routed, 'tp', axis=1, tiled=True)  16.7 us
    ppermute x7, starting transfers between devices, sent_to_each(): lax.ppermute(sent, axis, [(d, (d + far) % ways) for d in range(ways)])  9 us
    all_gather x1, blocking collectives, on_device(): mix_grad = lax.all_gather(grad_stream, 'tp', axis=1, tiled=True)  8.42 us
    ppermute x7, waiting for transfers between devices, sent_to_each(): lax.ppermute(sent, axis, [(d, (d + far) % ways) for d in range(ways)])  7.14 us
  transfers between devices with their start and end apart: 14, of which 6 were waited for; matrix products, arithmetic and copies ran while one was open for 14% of the time, Pallas kernels for 0%

profile of v1, /device:TPU:0, one launch (start us, length us, event | category | flops | bytes accessed | tf_op | source)
XLA Modules:
  0.0 247.8 jit_solution(7587946689600463595)
XLA Ops:
  8.1 0.8 copy.28
  9.2 0.9 reduce-window.6
  10.1 0.2 slice_reduce_fusion
  10.9 2.1 gather_fusion.1
  13.2 0.2 select_select_fusion
  13.4 21.6 %all_to_all.21 = bf16[8,60,512]{2,1,0:T(8,128)(2,1)S(1)} all-to-all(bf16[8,60,512]{2,1,0:T(8,128)(2,1)S(1)} %select_select_fusion), channel_id=1, replica_groups=mesh['sp'=8,'tp'=4] {'sp'}, dimensions={0} | all-to-all | bytes 983040 | tf_op jit(solution)/shard_map/all_to_all | solution.py:94
  35.1 0.9 all_to_all.15
  36.2 0.5 mul.442
  37.2 2.1 gather_fusion
  39.6 0.9 fusion.17
  40.5 2.4 collective-permute-start
  42.9 1.7 collective-permute-start.2
  44.6 1.5 collective-permute-start.3
  46.1 1.7 collective-permute-start.4
  47.9 0.7 collective-permute-start.5
  48.6 0.9 collective-permute-start.6
  49.5 5.0 %collective-permute-done.3 = bf16[60,512]{1,0:T(8,128)(2,1)S(1)} collective-permute-done((bf16[60,512]{1,0:T(8,128)(2,1)S(1)}, bf16[60,512]{1,0:T(8,128)(2,1)S(1)}, u32[]{:S(2)}, u32[]{:S(2)}) %collective-permute-start.3) | collective-permute-done | bytes 61472 | tf_op jit(solution)/shard_map/ppermute | solution.py:14
  54.5 2.1 collective-permute-done.4
  56.6 0.8 concatenate.9
  57.5 1.6 fusion.16
  59.1 0.2 reduce-scatter.3.cloned.1.call-start
  59.4 4.9 %fusion.6 = f32[480,896]{1,0:T(8,128)S(1)} fusion(bf16[480,2048]{1,0:T(8,128)(2,1)} %all-gather.6.cloned.1.call-done, bf16[1,896,2048]{2,1,0:T(8,128)(2,1)} %param.20), kind=kOutput, calls=%fused_computation.39 | convolution fusion | flops 1761607680 | bytes 7356416 | tf_op jit(solution)/shard_map/dot_general | solution.py:30
  64.3 16.7 %all-gather.4.cloned.1.call-done = bf16[480,2048]{1,0:T(8,128)(2,1)} async-done(((bf16[480,512]{1,0:T(8,128)(2,1)}), bf16[480,2048]{1,0:T(8,128)(2,1)}) %all-gather.4.cloned.1.call-update) | async-done | bytes 1966096 | tf_op jit(solution)/shard_map/all_gather | solution.py:99
  81.0 5.1 %multiply_convert_fusion.2 = (bf16[480,896]{1,0:T(8,128)(2,1)S(1)}, f32[480,896]{1,0:T(8,128)S(1)}) fusion(f32[480,896]{1,0:T(8,128)S(1)} %fusion.6, bf16[480,2048]{1,0:T(8,128)(2,1)} %all-gather.4.cloned.1.call-done, bf16[1,896,2048]{2,1,0:T(8,128)(2,1)} %param.22), kind=kOutput, calls=%fused_computation.48 | convolution fusion | flops 1764188160 | bytes 9936896 | tf_op jit(solution)/shard_map/dot_general | solution.py:39
  86.1 0.9 copy-done.18
  87.0 2.2 fusion
  89.2 2.3 fusion.2
  91.5 1.2 copy-done.17
  92.7 3.7 %add_convert_fusion = bf16[480,2048]{1,0:T(8,128)(2,1)} fusion(f32[480,2048]{1,0:T(8,128)S(1)} %fusion, bf16[1,896,2048]{2,1,0:T(8,128)(2,1)S(1)} %copy-done.10, f32[480,896]{1,0:T(8,128)S(1)} %fusion.6, f32[480,896]{1,0:T(8,128)S(1)} %get-tuple-element.52, f32[480,896]{1,0:T(8,128)S(1)} %fusion.2), kind=kOutput, calls=%fused_computation.32 | convolution fusion | flops 1767874560 | bytes 14729216 | tf_op jit(solution)/shard_map/dot_general | solution.py:50
  96.5 0.5 all-gather.8.cloned.1.call-update
  97.1 30.0 %reduce-scatter.3.cloned.1.call-done = bf16[480,512]{1,0:T(8,128)(2,1)} async-done(((bf16[480,2048]{1,0:T(8,128)(2,1)}), bf16[480,512]{1,0:T(8,128)(2,1)}) %reduce-scatter.3.cloned.1.call-update) | async-done | bytes 491536 | tf_op jit(solution)/shard_map/reduce_scatter | solution.py:104
  127.0 1.9 all_to_all.16
  128.9 5.5 %all-to-all-start.1 = ((bf16[8,60,512]{2,1,0:T(8,128)(2,1)}), bf16[8,60,512]{2,1,0:T(8,128)(2,1)S(1)}, u32[]{:S(2)}, u32[]{:S(2)}) async-start(bf16[8,60,512]{2,1,0:T(8,128)(2,1)} %all_to_all.16), calls=%async_computation.2 | async-start | bytes 1048576 | tf_op jit(solution)/shard_map/all_to_all | solution.py:110
  135.2 21.8 %all-to-all-done.1 = bf16[8,60,512]{2,1,0:T(8,128)(2,1)S(1)} async-done(((bf16[8,60,512]{2,1,0:T(8,128)(2,1)}), bf16[8,60,512]{2,1,0:T(8,128)(2,1)S(1)}, u32[]{:S(2)}, u32[]{:S(2)}) %all-to-all-start.1) | async-done | bytes 491552 | tf_op jit(solution)/shard_map/all_to_all | solution.py:110
  157.1 2.1 gather_fusion.2
  159.4 1.1 convert_reduce_fusion
  160.6 8.4 %all_gather.14 = bf16[192,2048]{1,0:T(8,128)(2,1)S(1)} all-gather(bf16[192,512]{1,0:T(8,128)(2,1)S(1)} %add_convert_fusion.1), channel_id=1, replica_groups=mesh['sp'=8,'tp'=4] {'tp'}, dimensions={1}, use_global_device_ids=true | all-gather | bytes 983040 | tf_op jit(solution)/shard_map/all_gather | solution.py:116
  169.0 2.3 convolution_convert_fusion
  171.3 0.8 copy-done.4
  172.2 0.7 copy-done.12
  172.9 6.0 %convert_bitcast_fusion = bf16[1,896,2048]{2,1,0:T(8,128)(2,1)} fusion(bf16[480,2048]{1,0:T(8,128)(2,1)S(1)} %copy-done.12, f32[480,896]{1,0:T(8,128)} %copy-done.17, f32[480,896]{1,0:T(8,128)} %copy-done.16), kind=kOutput, calls=%fused_computation.43 | convolution fusion | flops 1766023168 | bytes 9076736 | tf_op jit(solution)/shard_map/dot_general | solution.py:42
  178.9 2.5 fusion.123
  181.4 7.0 %all-reduce = (f32[192]{0:T(256)S(1)}, f32[192]{0:T(256)S(1)}) all-reduce(f32[192]{0:T(256)S(1)} %get-tuple-element.7, f32[192]{0:T(256)S(1)} %get-tuple-element.6), channel_id=1, replica_groups=mesh['sp'=8,'tp'=4] {'tp'}, use_global_device_ids=true, to_apply=%region_11.13 | all-reduce | flops 384 | bytes 3072 | tf_op jit(solution)/shard_map/psum | solution.py:137
  188.5 1.3 collective-permute-start.7
  189.8 5.5 %convert_bitcast_fusion.1 = bf16[1,896,2048]{2,1,0:T(8,128)(2,1)} fusion(bf16[480,896]{1,0:T(8,128)(2,1)S(1)} %copy-done.19, bf16[480,2048]{1,0:T(8,128)(2,1)} %all-gather.6.cloned.1.call-done), kind=kOutput, calls=%fused_computation.44 | convolution fusion | flops 1763442688 | bytes 6496256 | tf_op jit(solution)/shard_map/dot_general | solution.py:47
  195.4 2.5 %fusion.22 = bf16[192,512]{1,0:T(8,128)(2,1)} fusion(f32[192,512]{1,0:T(8,128)S(1)} %subtract_multiply_fusion, f32[30,512]{1,0:T(8,128)S(1)} %collective-permute-done.7, f32[512]{0:T(512)S(1)} %bitcast.85, f32[512]{0:T(512)S(1)} %bitcast.86, f32[512]{0:T(512)S(1)} %bitcast.88, f32[512]{0:T(512)S(1)} %bitcast.89, f32[512]{0:T(512)S(1)} %bitcast.90, ...), kind=kLoop, calls=%fused_computation.101 | loop fusion | flops 9043968 | bytes 714752 | tf_op jit(solution)/shard_map/convert_element_type | solution.py:150
  197.9 41.0 %reduce-scatter.5.cloned.1.call-done = bf16[256,512]{1,0:T(8,128)(2,1)} async-done(((bf16[2048,512]{1,0:T(8,128)(2,1)}), bf16[256,512]{1,0:T(8,128)(2,1)}) %reduce-scatter.5.cloned.1.call-update) | async-done | bytes 262160 | tf_op jit(solution)/shard_map/reduce_scatter | solution.py:128
  238.9 1.8 convert_element_type.72
  (92 shorter events, 3.5 us)
Async XLA Ops:
  8.0 2.9 %copy-start = (bf16[192,512]{1,0:T(8,128)(2,1)S(1)}, bf16[192,512]{1,0:T(8,128)(2,1)}, u32[]{:S(2)}) copy-start(bf16[192,512]{1,0:T(8,128)(2,1)} %param.16) | copy-start | bytes 589828
  8.0 51.4 %all-gather.6.cloned.1.call-start = ((), (), s32[]{:S(2)}) async-start(), calls=%async_computation.5 | async-start | bytes 2457600 | tf_op jit(solution)/shard_map/all_gather | solution.py:98
  13.1 22.9 %copy-start.1 = (bf16[192,512]{1,0:T(8,128)(2,1)S(1)}, bf16[192,512]{1,0:T(8,128)(2,1)}, u32[]{:S(2)}) copy-start(bf16[192,512]{1,0:T(8,128)(2,1)} %param.17) | copy-start | bytes 589828
  35.1 1.7 copy-start.6
  35.9 45.0 %all-gather.4.cloned.1.call-start = ((), (), s32[]{:S(2)}) async-start(), calls=%async_computation.4 | async-start | bytes 2457600 | tf_op jit(solution)/shard_map/all_gather | solution.py:99
  40.5 7.3 %collective-permute-start = (bf16[60,512]{1,0:T(8,128)(2,1)S(1)}, bf16[60,512]{1,0:T(8,128)(2,1)S(1)}, u32[]{:S(2)}, u32[]{:S(2)}) collective-permute-start(bf16[60,512]{1,0:T(8,128)(2,1)S(1)} %get-tuple-element.17), channel_id=1, source_target_pairs={{0,28},{4,0},{8,4},{12,8},{16,12},{20,16},{24,20},{28,24},{1,29},{... | collective-permute-start | bytes 184328 | tf_op jit(solution)/shard_map/ppermute | solution.py:14
  42.9 5.7 %collective-permute-start.1 = (bf16[60,512]{1,0:T(8,128)(2,1)S(1)}, bf16[60,512]{1,0:T(8,128)(2,1)S(1)}, u32[]{:S(2)}, u32[]{:S(2)}) collective-permute-start(bf16[60,512]{1,0:T(8,128)(2,1)S(1)} %get-tuple-element.16), channel_id=1, source_target_pairs={{0,24},{4,28},{8,0},{12,4},{16,8},{20,12},{24,16},{28,20},{1,25},{... | collective-permute-start | bytes 184328 | tf_op jit(solution)/shard_map/ppermute | solution.py:14
  42.9 6.6 %collective-permute-start.2 = (bf16[60,512]{1,0:T(8,128)(2,1)S(1)}, bf16[60,512]{1,0:T(8,128)(2,1)S(1)}, u32[]{:S(2)}, u32[]{:S(2)}) collective-permute-start(bf16[60,512]{1,0:T(8,128)(2,1)S(1)} %get-tuple-element.15), channel_id=1, source_target_pairs={{0,20},{4,24},{8,28},{12,0},{16,4},{20,8},{24,12},{28,16},{1,21},{... | collective-permute-start | bytes 184328 | tf_op jit(solution)/shard_map/ppermute | solution.py:14
  44.6 9.9 %collective-permute-start.3 = (bf16[60,512]{1,0:T(8,128)(2,1)S(1)}, bf16[60,512]{1,0:T(8,128)(2,1)S(1)}, u32[]{:S(2)}, u32[]{:S(2)}) collective-permute-start(bf16[60,512]{1,0:T(8,128)(2,1)S(1)} %get-tuple-element.14), channel_id=1, source_target_pairs={{0,16},{4,20},{8,24},{12,28},{16,0},{20,4},{24,8},{28,12},{1,17},{... | collective-permute-start | bytes 184328 | tf_op jit(solution)/shard_map/ppermute | solution.py:14
  46.1 10.5 %collective-permute-start.4 = (bf16[60,512]{1,0:T(8,128)(2,1)S(1)}, bf16[60,512]{1,0:T(8,128)(2,1)S(1)}, u32[]{:S(2)}, u32[]{:S(2)}) collective-permute-start(bf16[60,512]{1,0:T(8,128)(2,1)S(1)} %get-tuple-element.13), channel_id=1, source_target_pairs={{0,12},{4,16},{8,20},{12,24},{16,28},{20,0},{24,4},{28,8},{1,13},{... | collective-permute-start | bytes 184328 | tf_op jit(solution)/shard_map/ppermute | solution.py:14
  47.9 8.8 %collective-permute-start.5 = (bf16[60,512]{1,0:T(8,128)(2,1)S(1)}, bf16[60,512]{1,0:T(8,128)(2,1)S(1)}, u32[]{:S(2)}, u32[]{:S(2)}) collective-permute-start(bf16[60,512]{1,0:T(8,128)(2,1)S(1)} %get-tuple-element.12), channel_id=1, source_target_pairs={{0,8},{4,12},{8,16},{12,20},{16,24},{20,28},{24,0},{28,4},{1,9},{5... | collective-permute-start | bytes 184328 | tf_op jit(solution)/shard_map/ppermute | solution.py:14
  48.6 8.0 %collective-permute-start.6 = (bf16[60,512]{1,0:T(8,128)(2,1)S(1)}, bf16[60,512]{1,0:T(8,128)(2,1)S(1)}, u32[]{:S(2)}, u32[]{:S(2)}) collective-permute-start(bf16[60,512]{1,0:T(8,128)(2,1)S(1)} %get-tuple-element.11), channel_id=1, source_target_pairs={{0,4},{4,8},{8,12},{12,16},{16,20},{20,24},{24,28},{28,0},{1,5},{5... | collective-permute-start | bytes 184328 | tf_op jit(solution)/shard_map/ppermute | solution.py:14
  59.1 67.9 %reduce-scatter.3.cloned.1.call-start = ((), (), s32[]{:S(2)}) async-start(), calls=%async_computation.6 | async-start | bytes 2457600 | tf_op jit(solution)/shard_map/reduce_scatter | solution.py:104
  64.3 27.3 %copy-start.16 = (f32[480,896]{1,0:T(8,128)}, f32[480,896]{1,0:T(8,128)S(1)}, u32[]{:S(2)}) copy-start(f32[480,896]{1,0:T(8,128)S(1)} %fusion.6) | copy-start | bytes 5160964
  81.0 6.0 %copy-start.9 = (bf16[1,896,2048]{2,1,0:T(8,128)(2,1)S(1)}, bf16[1,896,2048]{2,1,0:T(8,128)(2,1)}, u32[]{:S(2)}) copy-start(bf16[1,896,2048]{2,1,0:T(8,128)(2,1)} %param.21) | copy-start | bytes 11010052
  86.1 0.9 copy-start.18
  87.0 2.2 copy-start.11
  89.2 3.5 %copy-start.10 = (bf16[1,896,2048]{2,1,0:T(8,128)(2,1)S(1)}, bf16[1,896,2048]{2,1,0:T(8,128)(2,1)}, u32[]{:S(2)}) copy-start(bf16[1,896,2048]{2,1,0:T(8,128)(2,1)} %param.20) | copy-start | bytes 11010052
  91.5 1.2 copy-start.17
  96.4 38.2 %copy-start.5 = (s32[192,2]{0,1:T(2,128)S(1)}, s32[192,2]{0,1:T(2,128)}, u32[]{:S(2)}) copy-start(s32[192,2]{0,1:T(2,128)} %param.18) | copy-start | bytes 4612
  96.5 82.4 %all-gather.8.cloned.1.call-start = ((), (), s32[]{:S(2)}) async-start(), calls=%async_computation.8 | async-start | bytes 2359296 | tf_op jit(solution)/shard_map/all_gather | solution.py:124
  128.9 28.1 %all-to-all-start.1 = ((bf16[8,60,512]{2,1,0:T(8,128)(2,1)}), bf16[8,60,512]{2,1,0:T(8,128)(2,1)S(1)}, u32[]{:S(2)}, u32[]{:S(2)}) async-start(bf16[8,60,512]{2,1,0:T(8,128)(2,1)} %all_to_all.16), calls=%async_computation.2 | async-start | bytes 1048576 | tf_op jit(solution)/shard_map/all_to_all | solution.py:110
  134.4 104.5 %reduce-scatter.5.cloned.1.call-start = ((), (), s32[]{:S(2)}) async-start(), calls=%async_computation.7 | async-start | bytes 2359296 | tf_op jit(solution)/shard_map/reduce_scatter | solution.py:128
  159.2 9.8 %copy-start.3 = (bf16[192,512]{1,0:T(8,128)(2,1)S(1)}, bf16[192,512]{1,0:T(8,128)(2,1)}, u32[]{:S(2)}) copy-start(bf16[192,512]{1,0:T(8,128)(2,1)} %param.23) | copy-start | bytes 589828
  159.2 9.8 %copy-start.7 = (f32[192]{0:T(256)S(1)}, f32[192]{0:T(256)}, u32[]{:S(2)}) copy-start(f32[192]{0:T(256)} %param.25) | copy-start | bytes 2308
  159.2 9.8 %copy-start.8 = (f32[192]{0:T(256)S(1)}, f32[192]{0:T(256)}, u32[]{:S(2)}) copy-start(f32[192]{0:T(256)} %param.24) | copy-start | bytes 2308
  159.2 9.8 %copy-start.13 = (f32[512]{0:T(512)S(1)}, f32[512]{0:T(512)}, u32[]{:S(2)}) copy-start(f32[512]{0:T(512)} %param.27) | copy-start | bytes 6148
  159.2 9.8 %copy-start.14 = (f32[512]{0:T(512)S(1)}, f32[512]{0:T(512)}, u32[]{:S(2)}) copy-start(f32[512]{0:T(512)} %param.26) | copy-start | bytes 6148
  160.6 10.7 %copy-start.2 = (bf16[192,512]{1,0:T(8,128)(2,1)}, bf16[192,512]{1,0:T(8,128)(2,1)S(1)}, u32[]{:S(2)}) copy-start(bf16[192,512]{1,0:T(8,128)(2,1)S(1)} %add_convert_fusion.1) | copy-start | bytes 589828
  171.3 0.8 copy-start.4
  171.3 1.6 copy-start.12
  172.9 6.0 %copy-start.15 = (f32[512]{0:T(512)S(1)}, f32[512]{0:T(512)}, u32[]{:S(2)}) copy-start(f32[512]{0:T(512)} %param.26) | copy-start | bytes 6148
  178.9 10.9 %copy-start.19 = (bf16[480,896]{1,0:T(8,128)(2,1)S(1)}, bf16[480,896]{1,0:T(8,128)(2,1)}, u32[]{:S(2)}) copy-start(bf16[480,896]{1,0:T(8,128)(2,1)} %copy-done.18) | copy-start | bytes 2580484
  188.5 6.9 %collective-permute-start.7 = (f32[30,512]{1,0:T(8,128)S(1)}, f32[30,512]{1,0:T(8,128)S(1)}, u32[]{:S(2)}, u32[]{:S(2)}) collective-permute-start(f32[30,512]{1,0:T(8,128)S(1)} %slice.303), channel_id=1, source_target_pairs={{4,0},{8,4},{12,8},{16,12},{20,16},{24,20},{28,24},{5,1},{9,5},{13... | collective-permute-start | bytes 184328 | tf_op jit(solution)/shard_map/ppermute | solution.py:22
Sparse Core Ops, SparseCore 0:
  36.1 20.8 all-gather.5
  59.3 21.6 all-gather.3
  96.6 30.3 reduce-scatter.2
Sparse Core Ops, SparseCore 1:
  99.1 58.3 all-gather.7
  171.4 67.5 reduce-scatter.4
